TPU v7x, 32 devices: a whole 2x2x4 slice. The times are simulated.
32 devices in a mesh: sp: 8 (over z, x), tp: 4 (over y, core).
Axes of the slice: x: 2, y: 2, z: 4, core: 2. Of those that a mesh axis runs over, the one named last changes fastest.
Arguments:
- inputs: bfloat16 [4096, 2048], P(('sp', 'tp')), may hold values from -6 to 6
- norm_gain: float32 [2048], replicated, may hold values from 0.1 to 1.9
- w_query: bfloat16 [2048, 1024], P(None, 'tp'), may hold values from -1 to 1
- w_key: bfloat16 [2048, 1024], P(None, 'tp'), may hold values from -1 to 1
- w_value: bfloat16 [2048, 1024], P(None, 'tp'), may hold values from -0.125 to 0.125
- query_gain: float32 [2, 64], replicated, may hold values from 1 to 5.5
- key_gain: float32 [2, 64], replicated, may hold values from 1 to 5.5
- lambdas: float32 [8], P('tp'), may hold values from 0.3 to 0.8
- sub_gain: float32 [128], replicated, may hold values from 0.1 to 1.9
- w_gate_b: bfloat16 [2048, 1024], P(None, 'tp'), may hold values from -0.125 to 0.125
- w_gate_c: bfloat16 [2048, 1024], P(None, 'tp'), may hold values from -0.125 to 0.125
- w_conv_in: bfloat16 [2048, 1024], P(None, 'tp'), may hold values from -0.125 to 0.125
- conv_taps: float32 [3, 1024], P(None, 'tp'), may hold values from -3 to 3
- conv_gain: float32 [1024], P('tp'), may hold values from 0.1 to 1.9
- w_out_att: bfloat16 [1024, 2048], P('tp'), may hold values from -0.125 to 0.125
- w_out_conv: bfloat16 [1024, 2048], P('tp'), may hold values from -0.125 to 0.125
Outputs:
- mixed: float32 [4096, 2048], P(('sp', 'tp'))
- log_sums: float32 [8, 2, 4096], P('tp', None, 'sp')
All inputs are finite; a program needn't handle non-finite values.
Results may differ from a plain program's by a relative error of at most 0.034.
Values may be sent and summed in bfloat16 or wider, within the bound.
A program may use at most 192 MiB of HBM per device.

v0:
```python
import math

import jax
import jax.numpy as jnp
from jax import lax
from jax.sharding import PartitionSpec as P

GROUP = 64


eps = 1e-06


def from_behind(shard, axis, by):
    count = lax.axis_size(axis)
    pairs = [(i, i + by) for i in range(count) if 0 <= i + by < count]
    return lax.ppermute(shard, axis, pairs)


def rms_scale(values):
    return values * lax.rsqrt(jnp.mean(values * values, axis=-1, keepdims=True) + eps)


def on_device(
    inputs,
    norm_gain,
    w_query,
    w_key,
    w_value,
    query_gain,
    key_gain,
    lambdas,
    sub_gain,
    w_gate_b,
    w_gate_c,
    w_conv_in,
    conv_taps,
    conv_gain,
    w_out_att,
    w_out_conv,
):
    heads_here = lambdas.shape[0]
    comp = query_gain.shape[1]
    vsize = sub_gain.shape[0]
    channels = conv_gain.shape[0]
    taps_count = conv_taps.shape[0]
    normed = (rms_scale(inputs.astype(jnp.float32)) * norm_gain).astype(jnp.bfloat16)
    attention_weights = (w_query, w_key, w_value)
    conv_weights = (w_gate_b, w_gate_c, w_conv_in)

    def dots(source, weights):
        return jnp.concatenate(
            [
                jnp.dot(source, weight, preferred_element_type=jnp.float32).astype(jnp.bfloat16)
                for weight in weights
            ],
            axis=1,
        )

    att_proj = dots(lax.all_gather(normed, "tp", axis=0, tiled=True), attention_weights)
    conv_proj = dots(lax.all_gather(normed, "tp", axis=0, tiled=True), conv_weights)
    rows = att_proj.shape[0]
    qcols = heads_here * 2 * comp
    query = att_proj[:, :qcols].reshape(rows, heads_here, 2, comp)
    key = att_proj[:, qcols : 2 * qcols].reshape(rows, heads_here, 2, comp)
    value = att_proj[:, 2 * qcols :]
    qn = (rms_scale(query.astype(jnp.float32)) * query_gain * comp ** (-0.5)).astype(jnp.bfloat16)
    kn = (rms_scale(key.astype(jnp.float32)) * key_gain).astype(jnp.bfloat16)
    stacked = jnp.stack([kn.reshape(rows, qcols), value], axis=0)
    position = lax.axis_index("sp")
    first_row = position * rows

    def make_absorb(queries, query_start):
        count_q = queries.shape[0]
        query_pos = query_start + jnp.arange(count_q, dtype=jnp.int32)
        last_query = query_start + count_q - 1

        def absorb(carry, piece, start):
            count = piece.shape[1]
            kblock = math.gcd(count, 512)

            def step(block, state):
                key_start = block * kblock

                def work(state):
                    top, total, acc = state
                    kv_rows = lax.dynamic_slice_in_dim(piece, block * kblock, kblock, 1)
                    kblk = kv_rows[0].reshape(kblock, heads_here, 2, comp)
                    vblk = kv_rows[1].reshape(kblock, heads_here, vsize)
                    scores = jnp.einsum(
                        "qhmd,khmd->hmqk", queries, kblk, preferred_element_type=jnp.float32
                    )
                    key_pos = key_start + jnp.arange(kblock, dtype=jnp.int32)
                    allowed = key_pos[None, :] <= query_pos[:, None]
                    scores = jnp.where(allowed, scores, -1e30)
                    top_new = jnp.maximum(top, jnp.max(scores, axis=-1))
                    prob = jnp.where(allowed, jnp.exp(scores - top_new[..., None]), 0.0)
                    factor = jnp.exp(top - top_new)
                    total = total * factor + jnp.sum(prob, axis=-1)
                    acc = acc * factor[..., None] + jnp.einsum(
                        "hmqk,khd->hmqd",
                        prob.astype(jnp.bfloat16),
                        vblk,
                        preferred_element_type=jnp.float32,
                    )
                    return (top_new, total, acc)

                return lax.cond(key_start <= last_query, work, lambda s: s, state)

            return lax.fori_loop(0, count // kblock, step, carry)

        return absorb

    def empty_state(count_q):
        return (
            jnp.full((heads_here, 2, count_q), -1e30, jnp.float32),
            jnp.zeros((heads_here, 2, count_q), jnp.float32),
            jnp.zeros((heads_here, 2, count_q, vsize), jnp.float32),
        )

    query_sets = ((qn, first_row),)
    absorbers = [make_absorb(queries, query_start) for queries, query_start in query_sets]
    initial = tuple((empty_state(queries.shape[0]) for queries, query_start in query_sets))
    piece = lax.all_gather(stacked, "sp", axis=1, tiled=True)
    start = jnp.int32(0)
    states = tuple(
        (absorber(carried, piece, start) for absorber, carried in zip(absorbers, initial))
    )
    top = jnp.concatenate([state[0] for state in states], axis=2)
    total = jnp.concatenate([state[1] for state in states], axis=2)
    acc = jnp.concatenate([state[2] for state in states], axis=2)
    map_out = acc / total[..., None]
    attn = map_out[:, 0] - lambdas[:, None, None] * map_out[:, 1]
    log_sums = top + jnp.log(total)
    heads_out = (
        (rms_scale(attn) * sub_gain)
        .astype(jnp.bfloat16)
        .transpose(1, 0, 2)
        .reshape(rows, heads_here * vsize)
    )
    gate_b = conv_proj[:, :channels].astype(jnp.float32)
    gate_c = conv_proj[:, channels : 2 * channels].astype(jnp.float32)
    conv_in = conv_proj[:, 2 * channels :].astype(jnp.float32)
    u_vals = (gate_c * conv_in).astype(jnp.bfloat16)
    edge = from_behind(u_vals[rows - (taps_count - 1) :], "sp", 1)
    padded = jnp.concatenate([edge, u_vals], axis=0).astype(jnp.float32)
    conv = conv_taps[0] * padded[0:rows]
    for tap in range(1, taps_count):
        conv = conv + conv_taps[tap] * padded[tap : tap + rows]
    gated = gate_b * conv
    grouped = rms_scale(gated.reshape(rows, channels // GROUP, GROUP)).reshape(rows, channels)
    conv_out = (grouped * conv_gain).astype(jnp.bfloat16)
    mixed = lax.psum_scatter(
        jnp.dot(heads_out, w_out_att, preferred_element_type=jnp.float32)
        + jnp.dot(conv_out, w_out_conv, preferred_element_type=jnp.float32),
        "tp",
        scatter_dimension=0,
        tiled=True,
    )
    return (mixed, log_sums)


def solution(mesh):
    in_specs = (
        P(("sp", "tp"), None),
        P(),
        P(None, "tp"),
        P(None, "tp"),
        P(None, "tp"),
        P(),
        P(),
        P("tp"),
        P(),
        P(None, "tp"),
        P(None, "tp"),
        P(None, "tp"),
        P(None, "tp"),
        P("tp"),
        P("tp", None),
        P("tp", None),
    )
    out_specs = (P(("sp", "tp"), None), P("tp", None, "sp"))
    return jax.shard_map(
        on_device, mesh=mesh, in_specs=in_specs, out_specs=out_specs, check_vma=False
    )
```

profile of v0, /device:TPU:24, one launch (start us, length us, event | category | flops | bytes accessed | tf_op | source)
XLA Modules:
  0.0 207.9 jit_solution(14211514563369810989)
XLA Ops:
  7.2 1.3 fusion.24
  8.5 2.0 fusion.26
  10.6 0.7 mul.199
  11.4 22.9 %all-gather.3.cloned.1.call-done = bf16[512,2048]{1,0:T(8,128)(2,1)} async-done(((bf16[128,2048]{1,0:T(8,128)(2,1)}), bf16[512,2048]{1,0:T(8,128)(2,1)}) %all-gather.3.cloned.1.call-update) | async-done | bytes 2097168 | tf_op jit(solution)/shard_map/all_gather | solution.py:60
  34.3 2.8 %bitcast_reduce_fusion.1 = (f32[512,2,2]{0,2,1:T(2,128)S(1)}, f32[512,256]{0,1:T(8,128)S(1)}) fusion(bf16[512,2048]{1,0:T(8,128)(2,1)} %all-gather.3.cloned.1.call-done, bf16[2048,256]{1,0:T(8,128)(2,1)} %param.23), kind=kOutput, calls=%fused_computation.64 | convolution fusion | flops 537393152 | bytes 3678208 | tf_op jit(solution)/shard_map/dot_general | solution.py:54
  37.2 0.8 fusion.23
  38.0 0.8 pad_maximum_fusion
  39.0 2.1 fusion.22
  41.1 2.1 fusion.21
  43.2 3.4 %collective-permute-start = (bf16[2,256]{0,1:T(8,128)(2,1)S(1)}, bf16[2,256]{0,1:T(8,128)(2,1)S(1)}, u32[]{:S(2)}, u32[]{:S(2)}) collective-permute-start(bf16[2,256]{0,1:T(8,128)(2,1)S(1)} %slice.44), channel_id=1, source_target_pairs={{0,4},{4,8},{8,12},{12,16},{16,20},{20,24},{24,28},{1,5},{5,9},{9,... | collective-permute-start | bytes 3080 | tf_op jit(solution)/shard_map/ppermute | solution.py:17
  46.6 0.8 fusion.27
  47.6 3.3 %collective-permute-done = bf16[2,256]{0,1:T(8,128)(2,1)S(1)} collective-permute-done((bf16[2,256]{0,1:T(8,128)(2,1)S(1)}, bf16[2,256]{0,1:T(8,128)(2,1)S(1)}, u32[]{:S(2)}, u32[]{:S(2)}) %collective-permute-start) | collective-permute-done | bytes 1056 | tf_op jit(solution)/shard_map/ppermute | solution.py:17
  51.0 0.9 bitcast_reduce_fusion
  51.9 0.8 fusion.36
  52.7 59.6 %all-gather.5.cloned.1.call-done = bf16[2,4096,256]{1,2,0:T(8,128)(2,1)} async-done(((bf16[2,512,256]{1,2,0:T(8,128)(2,1)}), bf16[2,4096,256]{1,2,0:T(8,128)(2,1)}) %all-gather.5.cloned.1.call-update) | async-done | bytes 4194320 | tf_op jit(solution)/shard_map/all_gather | solution.py:124
  112.4 34.4 %while.18 = (s32[]{:T(128)}, f32[2,2,512]{2,1,0:T(2,128)S(1)}, f32[2,2,512]{2,1,0:T(2,128)S(1)}, f32[2,2,512,128]{3,2,1,0:T(8,128)S(1)}, s32[]{:T(128)}, /*index...) while((s32[]{:T(128)}, f32[2,2,512]{2,1,0:T(2,128)S(1)}, ...), condition=%wide.region_8.9_spmd.clone, body=%wide.region_3.8_spmd.clone.sunk | while | flops 413930496 | bytes 17707344 | solution.py:110
  112.4 4.9 %conditional.3 = ((f32[2,2,512]{2,1,0:T(2,128)S(1)}, f32[2,2,512]{2,1,0:T(2,128)S(1)}, f32[2,2,512,128]{3,2,1,0:T(8,128)S(1)})) conditional(s32[]{:T(128)} %convert_element_type.152, (f32[2,2,512]{2,1,0:T(2,128)S(1)}, f32[2,2,512]{2,1,0:T(2,128)S(1)}, f32[2,2,512,128]{3,2,1,0:T(8,128)S(1)}) %tuple.55, (s32[]{:T(128)}, s32[]{:T(128)}, s32[]{:T(128)}, ...), branch_computations={%region_4.0_spmd, %region_5.7_spmd} | conditional | flops 413930496 | bytes 17705066 | solution.py:108
  112.5 0.2 broadcast_compare_fusion
  112.7 1.1 constant_dynamic-slice_fusion.1
  113.8 0.9 fusion.2
  114.6 0.9 fusion.4
  115.6 1.7 fusion.11
  117.3 4.9 %conditional.3 = ((f32[2,2,512]{2,1,0:T(2,128)S(1)}, f32[2,2,512]{2,1,0:T(2,128)S(1)}, f32[2,2,512,128]{3,2,1,0:T(8,128)S(1)})) conditional(s32[]{:T(128)} %convert_element_type.152, (f32[2,2,512]{2,1,0:T(2,128)S(1)}, f32[2,2,512]{2,1,0:T(2,128)S(1)}, f32[2,2,512,128]{3,2,1,0:T(8,128)S(1)}) %tuple.55, (s32[]{:T(128)}, s32[]{:T(128)}, s32[]{:T(128)}, ...), branch_computations={%region_4.0_spmd, %region_5.7_spmd} | conditional | flops 413930496 | bytes 17705066 | solution.py:108
  117.4 0.2 broadcast_compare_fusion
  117.6 1.1 constant_dynamic-slice_fusion.1
  118.7 0.9 fusion.2
  119.5 0.9 fusion.4
  120.5 1.7 fusion.11
  122.2 4.9 %conditional.3 = ((f32[2,2,512]{2,1,0:T(2,128)S(1)}, f32[2,2,512]{2,1,0:T(2,128)S(1)}, f32[2,2,512,128]{3,2,1,0:T(8,128)S(1)})) conditional(s32[]{:T(128)} %convert_element_type.152, (f32[2,2,512]{2,1,0:T(2,128)S(1)}, f32[2,2,512]{2,1,0:T(2,128)S(1)}, f32[2,2,512,128]{3,2,1,0:T(8,128)S(1)}) %tuple.55, (s32[]{:T(128)}, s32[]{:T(128)}, s32[]{:T(128)}, ...), branch_computations={%region_4.0_spmd, %region_5.7_spmd} | conditional | flops 413930496 | bytes 17705066 | solution.py:108
  122.3 0.2 broadcast_compare_fusion
  122.5 1.1 constant_dynamic-slice_fusion.1
  123.6 0.9 fusion.2
  124.4 0.9 fusion.4
  125.4 1.7 fusion.11
  127.1 4.9 %conditional.3 = ((f32[2,2,512]{2,1,0:T(2,128)S(1)}, f32[2,2,512]{2,1,0:T(2,128)S(1)}, f32[2,2,512,128]{3,2,1,0:T(8,128)S(1)})) conditional(s32[]{:T(128)} %convert_element_type.152, (f32[2,2,512]{2,1,0:T(2,128)S(1)}, f32[2,2,512]{2,1,0:T(2,128)S(1)}, f32[2,2,512,128]{3,2,1,0:T(8,128)S(1)}) %tuple.55, (s32[]{:T(128)}, s32[]{:T(128)}, s32[]{:T(128)}, ...), branch_computations={%region_4.0_spmd, %region_5.7_spmd} | conditional | flops 413930496 | bytes 17705066 | solution.py:108
  127.2 0.2 broadcast_compare_fusion
  127.4 1.1 constant_dynamic-slice_fusion.1
  128.5 0.9 fusion.2
  129.3 0.9 fusion.4
  130.3 1.7 fusion.11
  132.0 4.9 %conditional.3 = ((f32[2,2,512]{2,1,0:T(2,128)S(1)}, f32[2,2,512]{2,1,0:T(2,128)S(1)}, f32[2,2,512,128]{3,2,1,0:T(8,128)S(1)})) conditional(s32[]{:T(128)} %convert_element_type.152, (f32[2,2,512]{2,1,0:T(2,128)S(1)}, f32[2,2,512]{2,1,0:T(2,128)S(1)}, f32[2,2,512,128]{3,2,1,0:T(8,128)S(1)}) %tuple.55, (s32[]{:T(128)}, s32[]{:T(128)}, s32[]{:T(128)}, ...), branch_computations={%region_4.0_spmd, %region_5.7_spmd} | conditional | flops 413930496 | bytes 17705066 | solution.py:108
  132.1 0.2 broadcast_compare_fusion
  132.3 1.1 constant_dynamic-slice_fusion.1
  133.4 0.9 fusion.2
  134.2 0.9 fusion.4
  135.2 1.7 fusion.11
  136.9 4.9 %conditional.3 = ((f32[2,2,512]{2,1,0:T(2,128)S(1)}, f32[2,2,512]{2,1,0:T(2,128)S(1)}, f32[2,2,512,128]{3,2,1,0:T(8,128)S(1)})) conditional(s32[]{:T(128)} %convert_element_type.152, (f32[2,2,512]{2,1,0:T(2,128)S(1)}, f32[2,2,512]{2,1,0:T(2,128)S(1)}, f32[2,2,512,128]{3,2,1,0:T(8,128)S(1)}) %tuple.55, (s32[]{:T(128)}, s32[]{:T(128)}, s32[]{:T(128)}, ...), branch_computations={%region_4.0_spmd, %region_5.7_spmd} | conditional | flops 413930496 | bytes 17705066 | solution.py:108
  137.0 0.2 broadcast_compare_fusion
  137.2 1.1 constant_dynamic-slice_fusion.1
  138.3 0.9 fusion.2
  139.1 0.9 fusion.4
  140.1 1.7 fusion.11
  141.8 4.9 %conditional.3 = ((f32[2,2,512]{2,1,0:T(2,128)S(1)}, f32[2,2,512]{2,1,0:T(2,128)S(1)}, f32[2,2,512,128]{3,2,1,0:T(8,128)S(1)})) conditional(s32[]{:T(128)} %convert_element_type.152, (f32[2,2,512]{2,1,0:T(2,128)S(1)}, f32[2,2,512]{2,1,0:T(2,128)S(1)}, f32[2,2,512,128]{3,2,1,0:T(8,128)S(1)}) %tuple.55, (s32[]{:T(128)}, s32[]{:T(128)}, s32[]{:T(128)}, ...), branch_computations={%region_4.0_spmd, %region_5.7_spmd} | conditional | flops 413930496 | bytes 17705066 | solution.py:108
  141.9 0.2 broadcast_compare_fusion
  142.1 1.1 constant_dynamic-slice_fusion.1
  143.2 0.9 fusion.2
  144.0 0.9 fusion.4
  145.0 1.7 fusion.11
  146.8 0.3 copy.27
  147.8 0.7 fusion.40
  148.5 0.5 copy-done.2
  149.0 2.7 %convolution_add_fusion = f32[512,2048]{1,0:T(8,128)} fusion(f32[512,2048]{1,0:T(8,128)S(1)} %fusion.40, bf16[512,256]{0,1:T(8,128)(2,1)S(1)} %copy-done.3, bf16[256,2048]{1,0:T(8,128)(2,1)S(1)} %copy-done.2), kind=kOutput, calls=%fused_computation.21 | convolution fusion | flops 537919488 | bytes 9699328 | tf_op jit(solution)/shard_map/dot_general | solution.py:155
  151.8 0.6 log_add_fusion
  152.4 49.0 %reduce-scatter.2.cloned.1.call-done = f32[128,2048]{1,0:T(8,128)} async-done(((f32[512,2048]{1,0:T(8,128)}), f32[128,2048]{1,0:T(8,128)}) %reduce-scatter.2.cloned.1.call-update) | async-done | bytes 1048592 | tf_op jit(solution)/shard_map/reduce_scatter | solution.py:153
  (84 shorter events, 1.9 us)
Async XLA Ops:
  7.2 140.6 %copy-start = (bf16[256,2048]{1,0:T(8,128)(2,1)S(1)}, bf16[256,2048]{1,0:T(8,128)(2,1)}, u32[]{:S(2)}) copy-start(bf16[256,2048]{1,0:T(8,128)(2,1)} %param.34) | copy-start | bytes 3145732
  7.2 27.1 %all-gather.3.cloned.1.call-start = ((), (), s32[]{:S(2)}) async-start(), calls=%async_computation.1 | async-start | bytes 2621440 | tf_op jit(solution)/shard_map/all_gather | solution.py:60
  10.6 101.7 %all-gather.5.cloned.1.call-start = ((), (), s32[]{:S(2)}) async-start(), calls=%async_computation.2 | async-start | bytes 4718592 | tf_op jit(solution)/shard_map/all_gather | solution.py:124
  11.4 27.5 %copy-start.4 = (f32[3,256]{1,0:T(4,128)S(1)}, f32[3,256]{1,0:T(4,128)}, u32[]{:S(2)}) copy-start(f32[3,256]{1,0:T(4,128)} %param.32) | copy-start | bytes 9220
  34.3 2.9 %copy-start.1 = (bf16[512,2048]{1,0:T(8,128)(2,1)S(1)}, bf16[512,2048]{1,0:T(8,128)(2,1)}, u32[]{:S(2)}) copy-start(bf16[512,2048]{1,0:T(8,128)(2,1)} %all-gather.3.cloned.1.call-done) | copy-start | bytes 6291460
  34.3 2.9 %copy-start.9 = (bf16[2048,256]{1,0:T(8,128)(2,1)S(1)}, bf16[2048,256]{1,0:T(8,128)(2,1)}, u32[]{:S(2)}) copy-start(bf16[2048,256]{1,0:T(8,128)(2,1)} %param.24) | copy-start | bytes 3145732
  38.9 162.5 %reduce-scatter.2.cloned.1.call-start = ((), (), s32[]{:S(2)}) async-start(), calls=%async_computation.3 | async-start | bytes 5242880 | tf_op jit(solution)/shard_map/reduce_scatter | solution.py:153
  38.9 7.7 %copy-start.10 = (bf16[2048,256]{1,0:T(8,128)(2,1)S(1)}, bf16[2048,256]{1,0:T(8,128)(2,1)}, u32[]{:S(2)}) copy-start(bf16[2048,256]{1,0:T(8,128)(2,1)} %param.22) | copy-start | bytes 3145732
  41.0 6.4 %copy-start.6 = (f32[2,64]{1,0:T(2,128)S(1)}, f32[2,64]{1,0:T(2,128)}, u32[]{:S(2)}) copy-start(f32[2,64]{1,0:T(2,128)} %param.25) | copy-start | bytes 1540
  41.0 10.0 %copy-start.11 = (bf16[2048,256]{1,0:T(8,128)(2,1)S(1)}, bf16[2048,256]{1,0:T(8,128)(2,1)}, u32[]{:S(2)}) copy-start(bf16[2048,256]{1,0:T(8,128)(2,1)} %param.29) | copy-start | bytes 3145732
  43.2 8.7 %copy-start.7 = (f32[256]{0:T(256)S(1)}, f32[256]{0:T(256)}, u32[]{:S(2)}) copy-start(f32[256]{0:T(256)} %param.33) | copy-start | bytes 3076
  43.2 7.6 %collective-permute-start = (bf16[2,256]{0,1:T(8,128)(2,1)S(1)}, bf16[2,256]{0,1:T(8,128)(2,1)S(1)}, u32[]{:S(2)}, u32[]{:S(2)}) collective-permute-start(bf16[2,256]{0,1:T(8,128)(2,1)S(1)} %slice.44), channel_id=1, source_target_pairs={{0,4},{4,8},{8,12},{12,16},{16,20},{20,24},{24,28},{1,5},{5,9},{9,... | collective-permute-start | bytes 3080 | tf_op jit(solution)/shard_map/ppermute | solution.py:17
  146.8 0.7 copy-start.5
  146.8 0.8 copy-start.8
  147.8 1.2 copy-start.2
  147.8 1.3 copy-start.3
Sparse Core Ops, SparseCore 0:
  10.7 23.5 all-gather.2
  39.0 73.2 all-gather.4
  151.9 49.4 reduce-scatter.1
where the time goes:
time: 210 us; the launch traced here: 208 us
  waiting for transfers between devices  135 us (64%)
  matrix products  30.6 us (15%)
  other arithmetic  14.6 us (7%)
  between operations  14 us (7%)
  local copies, waits for them, and re-layouts  9.52 us (5%)
  starting transfers between devices  3.5 us (2%)
    all_gather x1, waiting for transfers between devices, on_device(): piece = lax.all_gather(stacked, 'sp', axis=1, tiled=True)  59.6 us
    reduce_scatter x1, waiting for transfers between devices, on_device(): lax.psum_scatter(jnp.dot(heads_out, w_out_att, preferred_element_type=jnp...  49 us
    all_gather x1, waiting for transfers between devices, on_device(): lax.all_gather(normed, 'tp', axis=0, tiled=True)  22.9 us
    dot_general x7, matrix products, work(): jnp.einsum('hmqk,khd->hmqd', prob.astype(jnp.bfloat16), vblk, preferred_e...  11.8 us
    dot_general x6, matrix products, dots(): jnp.dot(source, weight, preferred_element_type=jnp.float32)  9.31 us
    slice x7, local copies, waits for them, and re-layouts, work(): vblk = kv_rows[1].reshape(kblock, heads_here, vsize)  7.52 us
    reduce_sum x7, other arithmetic, work(): total = total * factor + jnp.sum(prob, axis=-1)  6.35 us
    dot_general x7, matrix products, work(): jnp.einsum('qhmd,khmd->hmqk', queries, kblk, preferred_element_type=jnp.f...  6.04 us
  transfers between devices with their start and end apart: 4, of which 4 were waited for; matrix products, arithmetic and copies ran while one was open for 4% of the time, Pallas kernels for 0%

commit v1 on v0

v1 whole, which is shorter than its diff:
```python
import functools

import jax
import jax.numpy as jnp
from jax import lax
from jax.experimental import pallas as pl
from jax.experimental.pallas import tpu as pltpu
from jax.sharding import PartitionSpec as P

GROUP = 64
eps = 1e-06
MESH = pl.DeviceIdType.MESH
VMEM_LIMIT = 60 * 1024 * 1024


def from_behind(shard, axis, by):
    count = lax.axis_size(axis)
    pairs = [(i, i + by) for i in range(count) if 0 <= i + by < count]
    return lax.ppermute(shard, axis, pairs)


def rms_scale(values):
    return values * lax.rsqrt(jnp.mean(values * values, axis=-1, keepdims=True) + eps)


def flip(index, bit):
    return index + bit - 2 * bit * lax.rem(index // bit, 2)


def remote(src, dst, send, recv, axis, target):
    return pltpu.make_async_remote_copy(
        src_ref=src,
        dst_ref=dst,
        send_sem=send,
        recv_sem=recv,
        device_id={axis: target},
        device_id_type=MESH,
    )


def greet(axis, targets):
    barrier = pltpu.get_barrier_semaphore()
    for target in targets:
        pl.semaphore_signal(barrier, inc=1, device_id={axis: target}, device_id_type=MESH)
    pl.semaphore_wait(barrier, len(targets))


CHUNKS = 4


def gather_project(x_ref, gain_ref, *rest):
    weights = rest[:6]
    att_ref, conv_ref, held, wbuf = rest[6:10]
    wsem, far_send, far_recv, near_sem, fwd_send, fwd_recv = rest[10:]
    me = lax.axis_index("tp")
    near, far = flip(me, 1), flip(me, 2)
    diag = flip(near, 2)
    rows = x_ref.shape[0]
    wcols = wbuf.shape[2]
    loads = [pltpu.make_async_copy(w, wbuf.at[i], wsem.at[i]) for i, w in enumerate(weights)]
    for load in loads:
        load.start()
    x = x_ref[...].astype(jnp.float32)
    held[me] = (rms_scale(x) * gain_ref[...]).astype(jnp.bfloat16)
    greet("tp", (near, far))
    part = rows // CHUNKS

    def far_copy(c):
        spot = held.at[me, pl.ds(c * part, part)]
        return remote(spot, spot, far_send.at[c], far_recv.at[c], "tp", far)

    def forward(c):
        spot = held.at[far, pl.ds(c * part, part)]
        return remote(spot, spot, fwd_send.at[c], fwd_recv.at[c], "tp", near)

    far_copies = [far_copy(c) for c in range(CHUNKS)]
    forwards = [forward(c) for c in range(CHUNKS)]
    near_copy = remote(held.at[me], held.at[me], near_sem.at[0], near_sem.at[1], "tp", near)
    for copy in far_copies:
        copy.start()
    near_copy.start()

    def project(slot):
        block = held[slot]
        at = pl.ds(pl.multiple_of(slot * rows, rows), rows)
        for i in range(6):
            out = att_ref if i < 3 else conv_ref
            out[at, (i % 3) * wcols : (i % 3 + 1) * wcols] = jnp.dot(
                block, wbuf[i], preferred_element_type=jnp.float32
            ).astype(jnp.bfloat16)

    for load in loads:
        load.wait()
    project(me)
    near_copy.wait_recv()
    project(near)
    for c in range(CHUNKS):
        far_copies[c].wait_recv()
        forwards[c].start()
    project(far)
    for copy in forwards:
        copy.wait_recv()
    project(diag)
    near_copy.wait_send()
    for copy in far_copies + forwards:
        copy.wait_send()


def attend(
    heads, q_ref, kv_ref, lam_ref, sub_ref, out_ref, log_ref, buf, qpad, top, total, acc,
    up_send, side_send, recv,
):
    n = buf.shape[0]
    me = lax.axis_index("sp")
    z, x = me // 2, lax.rem(me, 2)
    levels = n // 2
    partner = z * 2 + 1 - x
    rows = q_ref.shape[0]
    both = q_ref.shape[1] // heads
    comp = both // 2
    vsize = sub_ref.shape[0]
    barrier = pltpu.get_barrier_semaphore()
    has_up, has_down = z < levels - 1, z > 0
    pl.semaphore_signal(barrier, inc=1, device_id={"sp": partner}, device_id_type=MESH)

    @pl.when(has_up)
    def _():
        pl.semaphore_signal(barrier, inc=1, device_id={"sp": me + 2}, device_id_type=MESH)

    @pl.when(has_down)
    def _():
        pl.semaphore_signal(barrier, inc=1, device_id={"sp": me - 2}, device_id_type=MESH)

    pl.semaphore_wait(barrier, 1 + has_up.astype(jnp.int32) + has_down.astype(jnp.int32))

    def up_copy(src, block):
        return remote(
            src, buf.at[block], up_send.at[block // 2], recv.at[block], "sp",
            jnp.minimum(me + 2, n - 2 + x),
        )

    def side_copy(src, block):
        return remote(
            src, buf.at[block], side_send.at[block // 2], recv.at[block], "sp", partner
        )

    @pl.when(has_up)
    def _():
        up_copy(kv_ref, me).start()

    @pl.when(x == 0)
    def _():
        side_copy(kv_ref, me).start()

    lane = lax.broadcasted_iota(jnp.int32, (rows, both), 1)
    for h in range(heads):
        q = q_ref[:, h * both : (h + 1) * both]
        zero = jnp.zeros_like(q)
        qpad[h, :rows] = jnp.where(lane < comp, q, zero)
        qpad[h, rows:] = jnp.where(lane < comp, zero, q)
    top[...] = jnp.full_like(top, -1e30)
    total[...] = jnp.zeros_like(total)
    acc[...] = jnp.zeros_like(acc)
    tile = min(256, rows)

    def absorb(piece, masked):
        for h in range(heads):
            for start in range(0, 2 * rows, tile):
                first = start % rows
                keys = first + tile if masked else rows
                k = piece[:keys, h * both : (h + 1) * both]
                v = piece[:keys, heads * both + h * vsize : heads * both + (h + 1) * vsize]
                at = slice(start, start + tile)
                s = lax.dot_general(
                    k, qpad[h, at], (((1,), (1,)), ((), ())), preferred_element_type=jnp.float32
                )
                if masked:
                    kpos = lax.broadcasted_iota(jnp.int32, s.shape, 0)
                    qpos = first + lax.broadcasted_iota(jnp.int32, s.shape, 1)
                    s = jnp.where(kpos <= qpos, s, -1e30)
                old = top[h : h + 1, at]
                new = jnp.maximum(old, jnp.max(s, axis=0, keepdims=True))
                p = jnp.exp(s - new)
                factor = jnp.exp(old - new)
                top[h : h + 1, at] = new
                total[h : h + 1, at] = total[h : h + 1, at] * factor + jnp.sum(
                    p, axis=0, keepdims=True
                )
                acc[h, :, at] = acc[h, :, at] * factor + lax.dot_general(
                    v, p.astype(jnp.bfloat16), (((0,), (0,)), ((), ())),
                    preferred_element_type=jnp.float32,
                )

    absorb(kv_ref, True)

    @pl.loop(0, 2 * (z + 1))
    def _(j):
        step, other = j // 2 + 1, lax.rem(j, 2)
        level = z - step + other
        block = jnp.maximum(level, 0) * 2 + x + other * (1 - 2 * x)
        valid = jnp.where(other == 0, step <= z, (x == 1) | (step >= 2))

        @pl.when(valid)
        def _():
            side_copy(buf.at[block], block).wait_recv()

            @pl.when(other == 0)
            def _():
                @pl.when(has_up)
                def _():
                    up_copy(buf.at[block], block).start()

                side_copy(buf.at[block], block).start()

            absorb(buf.at[block], False)

    for h in range(heads):
        mapped = acc[h] / total[h : h + 1]
        attn = mapped[:, :rows] - lam_ref[h] * mapped[:, rows:]
        scale = lax.rsqrt(jnp.mean(attn * attn, axis=0, keepdims=True) + eps)
        result = attn * scale * sub_ref[...]
        out_ref[:, h * vsize : (h + 1) * vsize] = result.T.astype(jnp.bfloat16)
    log_ref[...] = top[...] + jnp.log(total[...])

    @pl.loop(0, z + 1)
    def _(level):
        block = level * 2 + x

        @pl.when(has_up)
        def _():
            up_copy(kv_ref, block).wait_send()

        @pl.when((x == 0) | (level < z))
        def _():
            side_copy(kv_ref, block).wait_send()


def project_scatter(
    heads_ref, conv_ref, wa_ref, wc_ref, out_ref, cross, fin, far, cross_in, fin_in, far_in,
    cross_send, cross_recv, fin_send, fin_recv, far_send, far_recv,
):
    me = lax.axis_index("tp")
    near, other = flip(me, 1), flip(me, 2)
    diag = flip(near, 2)
    rows = out_ref.shape[0]
    width = out_ref.shape[1] // CHUNKS
    greet("tp", (near, other))

    def partial(target, c):
        at = pl.ds(pl.multiple_of(target * rows, rows), rows)
        cols = slice(c * width, (c + 1) * width)
        return jnp.dot(
            heads_ref[at, :], wa_ref[:, cols], preferred_element_type=jnp.float32
        ) + jnp.dot(conv_ref[at, :], wc_ref[:, cols], preferred_element_type=jnp.float32)

    crosses = [
        remote(cross.at[c], cross_in.at[c], cross_send.at[c], cross_recv.at[c], "tp", near)
        for c in range(CHUNKS)
    ]
    fins = [
        remote(fin.at[c], fin_in.at[c], fin_send.at[c], fin_recv.at[c], "tp", near)
        for c in range(CHUNKS)
    ]
    fars = [
        remote(far.at[c], far_in.at[c], far_send.at[c], far_recv.at[c], "tp", other)
        for c in range(CHUNKS)
    ]
    for c in range(CHUNKS):
        cross[c] = partial(diag, c).astype(jnp.bfloat16)
        crosses[c].start()
    for c in range(CHUNKS):
        mine = partial(other, c)
        crosses[c].wait_recv()
        far[c] = (mine + cross_in[c].astype(jnp.float32)).astype(jnp.bfloat16)
        fars[c].start()
    for c in range(CHUNKS):
        fin[c] = partial(near, c).astype(jnp.bfloat16)
        fins[c].start()
    for c in range(CHUNKS):
        cols = slice(c * width, (c + 1) * width)
        out_ref[:, cols] = partial(me, c)
    for c in range(CHUNKS):
        cols = slice(c * width, (c + 1) * width)
        fins[c].wait_recv()
        fars[c].wait_recv()
        out_ref[:, cols] += fin_in[c].astype(jnp.float32) + far_in[c].astype(jnp.float32)
    for copy in crosses + fins + fars:
        copy.wait_send()


def vmem():
    return pl.BlockSpec(memory_space=pltpu.VMEM)


def on_device(
    inputs, norm_gain, w_query, w_key, w_value, query_gain, key_gain, lambdas, sub_gain,
    w_gate_b, w_gate_c, w_conv_in, conv_taps, conv_gain, w_out_att, w_out_conv,
):
    heads = lambdas.shape[0]
    comp = query_gain.shape[1]
    vsize = sub_gain.shape[0]
    channels = conv_gain.shape[0]
    taps_count = conv_taps.shape[0]
    own, width = inputs.shape
    tp = lax.axis_size("tp")
    sp = lax.axis_size("sp")
    rows = own * tp
    dma = pltpu.SemaphoreType.DMA

    def params(cid):
        return pltpu.CompilerParams(
            collective_id=cid, has_side_effects=True, vmem_limit_bytes=VMEM_LIMIT
        )

    qcols = heads * 2 * comp
    weights = (w_query, w_key, w_value, w_gate_b, w_gate_c, w_conv_in)
    att_proj, conv_proj = pl.pallas_call(
        gather_project,
        out_shape=(
            jax.ShapeDtypeStruct((rows, 3 * qcols), jnp.bfloat16),
            jax.ShapeDtypeStruct((rows, 3 * channels), jnp.bfloat16),
        ),
        in_specs=[vmem(), vmem()] + [pl.BlockSpec(memory_space=pl.ANY)] * 6,
        out_specs=(vmem(), vmem()),
        scratch_shapes=[
            pltpu.VMEM((tp, own, width), jnp.bfloat16),
            pltpu.VMEM((6, width, qcols), jnp.bfloat16),
            dma((6,)), dma((CHUNKS,)), dma((CHUNKS,)), dma((2,)), dma((CHUNKS,)), dma((CHUNKS,)),
        ],
        compiler_params=params(0),
        name="gather_project",
    )(inputs, norm_gain[None], *weights)

    query = att_proj[:, :qcols].reshape(rows, heads, 2, comp)
    key = att_proj[:, qcols : 2 * qcols].reshape(rows, heads, 2, comp)
    value = att_proj[:, 2 * qcols :]
    qn = (rms_scale(query.astype(jnp.float32)) * query_gain * comp ** (-0.5)).astype(jnp.bfloat16)
    kn = (rms_scale(key.astype(jnp.float32)) * key_gain).astype(jnp.bfloat16)
    kv = jnp.concatenate([kn.reshape(rows, qcols), value], axis=1)
    heads_out, logs = pl.pallas_call(
        functools.partial(attend, heads),
        out_shape=(
            jax.ShapeDtypeStruct((rows, heads * vsize), jnp.bfloat16),
            jax.ShapeDtypeStruct((heads, 2 * rows), jnp.float32),
        ),
        in_specs=[vmem(), vmem(), pl.BlockSpec(memory_space=pltpu.SMEM), vmem()],
        out_specs=(vmem(), vmem()),
        scratch_shapes=[
            pltpu.VMEM((sp, rows, kv.shape[1]), jnp.bfloat16),
            pltpu.VMEM((heads, 2 * rows, 2 * comp), jnp.bfloat16),
            pltpu.VMEM((heads, 2 * rows), jnp.float32),
            pltpu.VMEM((heads, 2 * rows), jnp.float32),
            pltpu.VMEM((heads, vsize, 2 * rows), jnp.float32),
            dma((sp // 2,)), dma((sp // 2,)), dma((sp,)),
        ],
        compiler_params=params(1),
        cost_estimate=pl.CostEstimate(flops=20_000_000_000, bytes_accessed=0, transcendentals=0),
        name="attend",
    )(qn.reshape(rows, qcols), kv, lambdas, sub_gain[:, None])
    log_sums = logs.reshape(heads, 2, rows)

    gate_b = conv_proj[:, :channels].astype(jnp.float32)
    gate_c = conv_proj[:, channels : 2 * channels].astype(jnp.float32)
    conv_in = conv_proj[:, 2 * channels :].astype(jnp.float32)
    u_vals = (gate_c * conv_in).astype(jnp.bfloat16)
    edge = from_behind(u_vals[rows - (taps_count - 1) :], "sp", 1)
    padded = jnp.concatenate([edge, u_vals], axis=0).astype(jnp.float32)
    conv = conv_taps[0] * padded[0:rows]
    for tap in range(1, taps_count):
        conv = conv + conv_taps[tap] * padded[tap : tap + rows]
    gated = gate_b * conv
    grouped = rms_scale(gated.reshape(rows, channels // GROUP, GROUP)).reshape(rows, channels)
    conv_out = (grouped * conv_gain).astype(jnp.bfloat16)

    piece = pltpu.VMEM((CHUNKS, own, width // CHUNKS), jnp.bfloat16)
    mixed = pl.pallas_call(
        project_scatter,
        out_shape=jax.ShapeDtypeStruct((own, width), jnp.float32),
        in_specs=[vmem()] * 4,
        out_specs=vmem(),
        scratch_shapes=[piece] * 6 + [dma((CHUNKS,))] * 6,
        compiler_params=params(2),
        name="project_scatter",
    )(heads_out, conv_out, w_out_att, w_out_conv)
    return (mixed, log_sums)


def solution(mesh):
    in_specs = (
        P(("sp", "tp"), None),
        P(),
        P(None, "tp"),
        P(None, "tp"),
        P(None, "tp"),
        P(),
        P(),
        P("tp"),
        P(),
        P(None, "tp"),
        P(None, "tp"),
        P(None, "tp"),
        P(None, "tp"),
        P("tp"),
        P("tp", None),
        P("tp", None),
    )
    out_specs = (P(("sp", "tp"), None), P("tp", None, "sp"))
    return jax.shard_map(
        on_device, mesh=mesh, in_specs=in_specs, out_specs=out_specs, check_vma=False
    )
```

time: 210 us -> 111 us (0.53)
  waiting for transfers between devices: 135 us -> 0.01 us
  Pallas kernels: 0 us -> 92.6 us
  matrix products: 30.6 us -> 0 us
  between operations: 14 us -> 0.86 us
  other arithmetic: 14.6 us -> 5.11 us
    pallas_call x0 -> x3, Pallas kernels: none -> 92.6 us  [the longest x1 55.2 us: on_device(): pl.pallas_call(functools.partial(attend, heads), out_shape=(jax.ShapeDtyp...]
    all_gather x2 -> x0, waiting for transfers between devices: 82.5 us -> none  [the longest x1 59.6 us: on_device(): piece = lax.all_gather(stacked, 'sp', axis=1, tiled=True)]
    reduce_scatter x1 -> x0, waiting for transfers between devices: 49 us -> none  [on_device(): lax.psum_scatter(jnp.dot(heads_out, w_out_att, preferred_element_type=jnp...]
    dot_general x22 -> x0, matrix products: 30.6 us -> none  [the longest x7 11.8 us: work(): jnp.einsum('hmqk,khd->hmqd', prob.astype(jnp.bfloat16), vblk, preferred_e...]
    slice x7 -> x1, local copies, waits for them, and re-layouts: 7.52 us -> 0.02 us  [on_device(): value = att_proj[:, 2 * qcols:]]
    reduce_sum x7 -> x0, other arithmetic: 6.35 us -> none  [work(): total = total * factor + jnp.sum(prob, axis=-1)]
    unnamed x24 -> x13, local copies, waits for them, and re-layouts: 0.69 us -> 4.7 us
    ppermute x1, waiting for transfers between devices: 3.3 us -> 0.01 us  [from_behind(): return lax.ppermute(shard, axis, pairs)]
  transfers between devices with their start and end apart: 4 -> 1, of which waited for: 4 -> 0; matrix products, arithmetic and copies ran while one was open for 4% -> 5% of each run, Pallas kernels for 0% -> 50%
where the time goes in v1:
time: 111 us; the launch traced here: 110 us
  Pallas kernels  92.6 us (83%)
  local copies, waits for them, and re-layouts  8.27 us (7%)
  other arithmetic  5.11 us (5%)
  starting transfers between devices  3.4 us (3%)
    pallas_call x1, Pallas kernels, on_device(): pl.pallas_call(functools.partial(attend, heads), out_shape=(jax.ShapeDtyp...  55.2 us
    pallas_call x1, Pallas kernels, on_device(): pl.pallas_call(gather_project, out_shape=(jax.ShapeDtypeStruct((rows, 3 *...  18.8 us
    pallas_call x1, Pallas kernels, on_device(): pl.pallas_call(project_scatter, out_shape=jax.ShapeDtypeStruct((own, widt...  18.7 us
    unnamed x13, local copies, waits for them, and re-layouts  4.7 us
    ppermute x1, starting transfers between devices, from_behind(): return lax.ppermute(shard, axis, pairs)  3.4 us
  transfers between devices with their start and end apart: 1, of which 0 were waited for; matrix products, arithmetic and copies ran while one was open for 5% of the time, Pallas kernels for 50%

profile of v1, /device:TPU:24, one launch (start us, length us, event | category | flops | bytes accessed | tf_op | source)
XLA Modules:
  0.0 110.2 jit_solution(13859658483166728492)
XLA Ops:
  0.6 18.8 %gather_project.1 = (bf16[512,768]{1,0:T(8,128)(2,1)}, bf16[512,768]{1,0:T(8,128)(2,1)}) custom-call(bf16[128,2048]{1,0:T(8,128)(2,1)} %x_ref.1, f32[1,2048]{1,0:T(1,128)} %bitcast.17, bf16[2048,256]{1,0:T(8,128)(2,1)} %rest_0_.1, bf16[2048,256]{1,0:T(8,128)(2,1)} %rest_1_.1, bf16[2048,256]{1,0:T(8,128)(2,1)} %rest_2_.1, bf16[2048,256]{1,0:T(8,128)(2,1)} %rest_3_.1, ...), custom_call_target="tpu_custom_call" | custom-call | tf_op jit(solution)/shard_map/gather_project/pallas_call | solution.py:317
  19.4 0.0 copy-start
  19.4 1.2 %multiply_convert_fusion.1 = bf16[512,256]{1,0:T(8,128)(2,1)S(1)} fusion(bf16[512,768]{1,0:T(8,128)(2,1)} %get-tuple-element.8), kind=kLoop, calls=%fused_computation.20 | loop fusion | flops 524288 | bytes 786432 | tf_op jit(solution)/shard_map/convert_element_type | solution.py:365
  20.6 3.4 %collective-permute-start = (bf16[2,256]{1,0:T(2,128)(2,1)S(1)}, bf16[2,256]{1,0:T(2,128)(2,1)S(1)}, u32[]{:S(2)}, u32[]{:S(2)}) collective-permute-start(bf16[2,256]{1,0:T(2,128)(2,1)S(1)} %slice.52), channel_id=1, source_target_pairs={{0,4},{4,8},{8,12},{12,16},{16,20},{20,24},{24,28},{1,5},{5,9},{9,... | collective-permute-start | bytes 3080 | tf_op jit(solution)/shard_map/ppermute | solution.py:19
  24.0 0.0 copy-done
  24.0 0.1 convert_multiply_fusion.1
  24.1 0.2 copy.21
  24.3 0.1 bitcast_reduce_fusion.1
  24.4 0.1 mul.141
  24.5 0.0 copy-start.2
  24.5 0.2 copy.22
  24.7 0.5 copy-done.2
  25.2 0.0 copy-start.3
  25.2 0.1 mul.145
  25.2 0.6 copy-done.3
  25.8 0.1 mul.134
  25.9 0.2 copy.19
  26.1 0.1 bitcast_reduce_fusion.2
  26.2 0.1 mul.130
  26.3 0.2 copy.20
  26.5 0.0 copy-start.5
  26.5 0.6 copy-done.5
  27.1 0.7 copy.23.sub_ref
  27.9 0.8 fusion.4
  28.7 0.8 pad_maximum_fusion.kv_ref
  29.5 0.0 copy-start.1
  29.5 55.2 %attend.1 = (bf16[512,256]{1,0:T(8,128)(2,1)}, f32[2,1024]{1,0:T(2,128)}) custom-call(bf16[512,256]{1,0:T(8,128)(2,1)} %get-tuple-element.13.q_ref, bf16[512,512]{1,0:T(8,128)(2,1)} %pad_maximum_fusion.kv_ref, f32[2]{0:T(128)} %lam_ref.1, f32[128,1]{1,0:T(8,128)} %copy.23.sub_ref), custom_call_target="tpu_custom_call" | custom-call | flops 20000000000 | tf_op jit(solution)/shard_map/attend/pallas_call | solution.py:340
  84.7 0.0 copy-done.1
  84.7 1.3 %reshape.50 = f32[2,2,512]{2,1,0:T(2,128)} reshape(f32[2,1024]{1,0:T(2,128)} %get-tuple-element.9) | data formatting | bytes 16384 | tf_op jit(solution)/shard_map/reshape | solution.py:360
  86.0 0.0 collective-permute-done
  86.0 0.1 maximum_convert_fusion
  86.1 1.2 %fusion.8 = (f32[512,256]{1,0:T(8,128)S(1)}, f32[512,256]{1,0:T(8,128)S(1)}) fusion(f32[514,256]{1,0:T(8,128)S(1)} %maximum_convert_fusion, f32[256]{0:T(256)S(1)} %bitcast.19, f32[256]{0:T(256)S(1)} %bitcast.20, f32[256]{0:T(256)S(1)} %bitcast.18, bf16[512,768]{1,0:T(8,128)(2,1)} %get-tuple-element.8), kind=kLoop, calls=%fused_computation.25 | loop fusion | flops 1048576 | bytes 2886656 | tf_op jit(solution)/shard_map/mul | solution.py:23
  87.3 0.2 copy.24
  87.5 0.1 bitcast_reduce_fusion
  87.5 0.1 mul.161
  87.6 0.2 copy.25
  87.8 0.0 copy-start.4
  87.8 0.7 copy-done.4
  88.5 0.8 multiply_convert_fusion.conv_ref
  89.3 18.7 %project_scatter.1 = f32[128,2048]{1,0:T(8,128)} custom-call(bf16[512,256]{1,0:T(8,128)(2,1)} %get-tuple-element.7.heads_ref, bf16[512,256]{1,0:T(8,128)(2,1)} %multiply_convert_fusion.conv_ref, bf16[256,2048]{1,0:T(8,128)(2,1)} %wa_ref.1, bf16[256,2048]{1,0:T(8,128)(2,1)} %wc_ref.1), custom_call_target="tpu_custom_call" | custom-call | tf_op jit(solution)/shard_map/project_scatter/pallas_call | solution.py:376
  107.9 2.3 %copy.27 = f32[128,2048]{1,0:T(8,128)} copy(f32[128,2048]{1,0:T(8,128)} %project_scatter.1) | data formatting | bytes 2097152
  (8 shorter events, 0.1 us)
Async XLA Ops:
  19.4 4.6 %copy-start = (bf16[512,768]{1,0:T(8,128)(2,1)S(1)}, bf16[512,768]{1,0:T(8,128)(2,1)}, u32[]{:S(2)}) copy-start(bf16[512,768]{1,0:T(8,128)(2,1)} %get-tuple-element.6) | copy-start | bytes 2359300
  20.6 65.4 %collective-permute-start = (bf16[2,256]{1,0:T(2,128)(2,1)S(1)}, bf16[2,256]{1,0:T(2,128)(2,1)S(1)}, u32[]{:S(2)}, u32[]{:S(2)}) collective-permute-start(bf16[2,256]{1,0:T(2,128)(2,1)S(1)} %slice.52), channel_id=1, source_target_pairs={{0,4},{4,8},{8,12},{12,16},{16,20},{20,24},{24,28},{1,5},{5,9},{9,... | collective-permute-start | bytes 3080 | tf_op jit(solution)/shard_map/ppermute | solution.py:19
  24.5 0.7 copy-start.2
  25.2 0.7 copy-start.3
  26.5 0.7 copy-start.5
  29.5 55.2 %copy-start.1 = (f32[3,256]{1,0:T(4,128)S(1)}, f32[3,256]{1,0:T(4,128)}, u32[]{:S(2)}) copy-start(f32[3,256]{1,0:T(4,128)} %param.28) | copy-start | bytes 9220
  87.8 0.7 copy-start.4

commit v2 on v1

--- a/solution.py
+++ b/solution.py
@@ -11,12 +11,6 @@
 eps = 1e-06
 MESH = pl.DeviceIdType.MESH
 VMEM_LIMIT = 60 * 1024 * 1024
-
-
-def from_behind(shard, axis, by):
-    count = lax.axis_size(axis)
-    pairs = [(i, i + by) for i in range(count) if 0 <= i + by < count]
-    return lax.ppermute(shard, axis, pairs)
 
 
 def rms_scale(values):
@@ -46,12 +40,27 @@
 
 
 CHUNKS = 4
-
-
-def gather_project(x_ref, gain_ref, *rest):
+HALVES = 2
+
+
+def group_scale(values, size):
+    lanes = values.shape[1]
+    row = lax.broadcasted_iota(jnp.int32, (lanes, lanes), 0) // size
+    col = lax.broadcasted_iota(jnp.int32, (lanes, lanes), 1) // size
+    ones = jnp.where(row == col, 1.0, 0.0).astype(jnp.bfloat16)
+    squares = values * values
+    high = squares.astype(jnp.bfloat16)
+    low = (squares - high.astype(jnp.float32)).astype(jnp.bfloat16)
+    sums = jnp.dot(high, ones, preferred_element_type=jnp.float32) + jnp.dot(
+        low, ones, preferred_element_type=jnp.float32
+    )
+    return lax.rsqrt(sums * (1.0 / size) + eps)
+
+
+def gather_project(comp, x_ref, gain_ref, qk_ref, *rest):
     weights = rest[:6]
-    att_ref, conv_ref, held, wbuf = rest[6:10]
-    wsem, far_send, far_recv, near_sem, fwd_send, fwd_recv = rest[10:]
+    q_ref, kv_ref, conv_ref, held, wbuf = rest[6:11]
+    wsem, far_send, far_recv, near_sem, fwd_send, fwd_recv = rest[11:]
     me = lax.axis_index("tp")
     near, far = flip(me, 1), flip(me, 2)
     diag = flip(near, 2)
@@ -84,10 +93,17 @@
         block = held[slot]
         at = pl.ds(pl.multiple_of(slot * rows, rows), rows)
         for i in range(6):
-            out = att_ref if i < 3 else conv_ref
-            out[at, (i % 3) * wcols : (i % 3 + 1) * wcols] = jnp.dot(
-                block, wbuf[i], preferred_element_type=jnp.float32
-            ).astype(jnp.bfloat16)
+            res = jnp.dot(block, wbuf[i], preferred_element_type=jnp.float32).astype(jnp.bfloat16)
+            if i < 2:
+                wide = res.astype(jnp.float32)
+                wide = wide * group_scale(wide, comp) * qk_ref[i : i + 1]
+                res = wide.astype(jnp.bfloat16)
+            if i == 0:
+                q_ref[at, :] = res
+            elif i < 3:
+                kv_ref[at, (i - 1) * wcols : i * wcols] = res
+            else:
+                conv_ref[at, (i - 3) * wcols : (i - 2) * wcols] = res
 
     for load in loads:
         load.wait()
@@ -107,8 +123,8 @@
 
 
 def attend(
-    heads, q_ref, kv_ref, lam_ref, sub_ref, out_ref, log_ref, buf, qpad, top, total, acc,
-    up_send, side_send, recv,
+    heads, q_ref, kv_ref, lam_ref, sub_ref, proj_ref, taps_ref, cgain_ref, out_ref, log_ref,
+    conv_ref, buf, qpad, top, total, acc, tail, padded, up_send, side_send, recv, tail_sem,
 ):
     n = buf.shape[0]
     me = lax.axis_index("sp")
@@ -131,26 +147,52 @@
     def _():
         pl.semaphore_signal(barrier, inc=1, device_id={"sp": me - 2}, device_id_type=MESH)
 
-    pl.semaphore_wait(barrier, 1 + has_up.astype(jnp.int32) + has_down.astype(jnp.int32))
-
-    def up_copy(src, block):
+    ups, downs = has_up.astype(jnp.int32), has_down.astype(jnp.int32)
+
+    @pl.when((x == 1) & has_up)
+    def _():
+        pl.semaphore_signal(barrier, inc=1, device_id={"sp": me + 1}, device_id_type=MESH)
+
+    @pl.when((x == 0) & has_down)
+    def _():
+        pl.semaphore_signal(barrier, inc=1, device_id={"sp": me - 1}, device_id_type=MESH)
+
+    pl.semaphore_wait(barrier, 1 + ups + downs + x * ups + (1 - x) * downs)
+    edge = tail.shape[0]
+    channels = conv_ref.shape[1]
+    tail_copy = remote(
+        proj_ref.at[pl.ds(rows - edge, edge), pl.ds(channels, 2 * channels)], tail,
+        tail_sem.at[0], tail_sem.at[1], "sp", jnp.minimum(me + 1, n - 1),
+    )
+    size = rows // HALVES
+
+    def up_copy(src, block, half):
+        at = pl.ds(half * size, size)
         return remote(
-            src, buf.at[block], up_send.at[block // 2], recv.at[block], "sp",
-            jnp.minimum(me + 2, n - 2 + x),
+            src.at[at], buf.at[block, at], up_send.at[block // 2, half], recv.at[block, half],
+            "sp", jnp.minimum(me + 2, n - 2 + x),
         )
 
-    def side_copy(src, block):
+    def side_copy(src, block, half):
+        at = pl.ds(half * size, size)
         return remote(
-            src, buf.at[block], side_send.at[block // 2], recv.at[block], "sp", partner
+            src.at[at], buf.at[block, at], side_send.at[block // 2, half], recv.at[block, half],
+            "sp", partner,
         )
 
     @pl.when(has_up)
     def _():
-        up_copy(kv_ref, me).start()
+        for half in range(HALVES):
+            up_copy(kv_ref, me, half).start()
 
     @pl.when(x == 0)
     def _():
-        side_copy(kv_ref, me).start()
+        for half in range(HALVES):
+            side_copy(kv_ref, me, half).start()
+
+    @pl.when(me < n - 1)
+    def _():
+        tail_copy.start()
 
     lane = lax.broadcasted_iota(jnp.int32, (rows, both), 1)
     for h in range(heads):
@@ -193,6 +235,30 @@
 
     absorb(kv_ref, True)
 
+    def product(ref, at):
+        gate = ref[:, at : at + channels].astype(jnp.float32)
+        other = ref[:, at + channels : at + 2 * channels].astype(jnp.float32)
+        return (gate * other).astype(jnp.bfloat16).astype(jnp.float32)
+
+    padded[edge:] = product(proj_ref, channels)
+
+    @pl.when(me > 0)
+    def _():
+        tail_copy.wait_recv()
+        padded[:edge] = product(tail, 0)
+
+    @pl.when(me == 0)
+    def _():
+        padded[:edge] = jnp.zeros((edge, channels), jnp.float32)
+
+    count = taps_ref.shape[0]
+    conv = jnp.zeros((rows, channels), jnp.float32)
+    for tap in range(count):
+        first = edge - count + 1 + tap
+        conv = conv + taps_ref[tap : tap + 1] * padded[first : first + rows]
+    gated = proj_ref[:, :channels].astype(jnp.float32) * conv
+    conv_ref[...] = (gated * group_scale(gated, GROUP) * cgain_ref[...]).astype(jnp.bfloat16)
+
     @pl.loop(0, 2 * (z + 1))
     def _(j):
         step, other = j // 2 + 1, lax.rem(j, 2)
@@ -202,15 +268,16 @@
 
         @pl.when(valid)
         def _():
-            side_copy(buf.at[block], block).wait_recv()
-
-            @pl.when(other == 0)
-            def _():
-                @pl.when(has_up)
+            for half in range(HALVES):
+                side_copy(buf.at[block], block, half).wait_recv()
+
+                @pl.when(other == 0)
                 def _():
-                    up_copy(buf.at[block], block).start()
-
-                side_copy(buf.at[block], block).start()
+                    @pl.when(has_up)
+                    def _():
+                        up_copy(buf.at[block], block, half).start()
+
+                    side_copy(buf.at[block], block, half).start()
 
             absorb(buf.at[block], False)
 
@@ -220,7 +287,9 @@
         scale = lax.rsqrt(jnp.mean(attn * attn, axis=0, keepdims=True) + eps)
         result = attn * scale * sub_ref[...]
         out_ref[:, h * vsize : (h + 1) * vsize] = result.T.astype(jnp.bfloat16)
-    log_ref[...] = top[...] + jnp.log(total[...])
+        logs = top[h : h + 1] + jnp.log(total[h : h + 1])
+        log_ref[h, 0:1, :] = logs[:, :rows]
+        log_ref[h, 1:2, :] = logs[:, rows:]
 
     @pl.loop(0, z + 1)
     def _(level):
@@ -228,11 +297,17 @@
 
         @pl.when(has_up)
         def _():
-            up_copy(kv_ref, block).wait_send()
+            for half in range(HALVES):
+                up_copy(kv_ref, block, half).wait_send()
 
         @pl.when((x == 0) | (level < z))
         def _():
-            side_copy(kv_ref, block).wait_send()
+            for half in range(HALVES):
+                side_copy(kv_ref, block, half).wait_send()
+
+    @pl.when(me < n - 1)
+    def _():
+        tail_copy.wait_send()
 
 
 def project_scatter(
@@ -300,7 +375,6 @@
     comp = query_gain.shape[1]
     vsize = sub_gain.shape[0]
     channels = conv_gain.shape[0]
-    taps_count = conv_taps.shape[0]
     own, width = inputs.shape
     tp = lax.axis_size("tp")
     sp = lax.axis_size("sp")
@@ -314,14 +388,21 @@
 
     qcols = heads * 2 * comp
     weights = (w_query, w_key, w_value, w_gate_b, w_gate_c, w_conv_in)
-    att_proj, conv_proj = pl.pallas_call(
-        gather_project,
+    qk_gain = jnp.stack(
+        [
+            jnp.tile(query_gain.reshape(-1) * comp ** (-0.5), heads),
+            jnp.tile(key_gain.reshape(-1), heads),
+        ]
+    )
+    qn, kv, conv_proj = pl.pallas_call(
+        functools.partial(gather_project, comp),
         out_shape=(
-            jax.ShapeDtypeStruct((rows, 3 * qcols), jnp.bfloat16),
+            jax.ShapeDtypeStruct((rows, qcols), jnp.bfloat16),
+            jax.ShapeDtypeStruct((rows, 2 * qcols), jnp.bfloat16),
             jax.ShapeDtypeStruct((rows, 3 * channels), jnp.bfloat16),
         ),
-        in_specs=[vmem(), vmem()] + [pl.BlockSpec(memory_space=pl.ANY)] * 6,
-        out_specs=(vmem(), vmem()),
+        in_specs=[vmem()] * 3 + [pl.BlockSpec(memory_space=pl.ANY)] * 6,
+        out_specs=(vmem(), vmem(), vmem()),
         scratch_shapes=[
             pltpu.VMEM((tp, own, width), jnp.bfloat16),
             pltpu.VMEM((6, width, qcols), jnp.bfloat16),
@@ -329,48 +410,31 @@
         ],
         compiler_params=params(0),
         name="gather_project",
-    )(inputs, norm_gain[None], *weights)
-
-    query = att_proj[:, :qcols].reshape(rows, heads, 2, comp)
-    key = att_proj[:, qcols : 2 * qcols].reshape(rows, heads, 2, comp)
-    value = att_proj[:, 2 * qcols :]
-    qn = (rms_scale(query.astype(jnp.float32)) * query_gain * comp ** (-0.5)).astype(jnp.bfloat16)
-    kn = (rms_scale(key.astype(jnp.float32)) * key_gain).astype(jnp.bfloat16)
-    kv = jnp.concatenate([kn.reshape(rows, qcols), value], axis=1)
-    heads_out, logs = pl.pallas_call(
+    )(inputs, norm_gain[None], qk_gain, *weights)
+
+    heads_out, log_sums, conv_out = pl.pallas_call(
         functools.partial(attend, heads),
         out_shape=(
             jax.ShapeDtypeStruct((rows, heads * vsize), jnp.bfloat16),
-            jax.ShapeDtypeStruct((heads, 2 * rows), jnp.float32),
+            jax.ShapeDtypeStruct((heads, 2, rows), jnp.float32),
+            jax.ShapeDtypeStruct((rows, channels), jnp.bfloat16),
         ),
-        in_specs=[vmem(), vmem(), pl.BlockSpec(memory_space=pltpu.SMEM), vmem()],
-        out_specs=(vmem(), vmem()),
+        in_specs=[vmem(), vmem(), pl.BlockSpec(memory_space=pltpu.SMEM)] + [vmem()] * 4,
+        out_specs=(vmem(), vmem(), vmem()),
         scratch_shapes=[
             pltpu.VMEM((sp, rows, kv.shape[1]), jnp.bfloat16),
             pltpu.VMEM((heads, 2 * rows, 2 * comp), jnp.bfloat16),
             pltpu.VMEM((heads, 2 * rows), jnp.float32),
             pltpu.VMEM((heads, 2 * rows), jnp.float32),
             pltpu.VMEM((heads, vsize, 2 * rows), jnp.float32),
-            dma((sp // 2,)), dma((sp // 2,)), dma((sp,)),
+            pltpu.VMEM((16, 2 * channels), jnp.bfloat16),
+            pltpu.VMEM((16 + rows, channels), jnp.float32),
+            dma((sp // 2, HALVES)), dma((sp // 2, HALVES)), dma((sp, HALVES)), dma((2,)),
         ],
         compiler_params=params(1),
         cost_estimate=pl.CostEstimate(flops=20_000_000_000, bytes_accessed=0, transcendentals=0),
         name="attend",
-    )(qn.reshape(rows, qcols), kv, lambdas, sub_gain[:, None])
-    log_sums = logs.reshape(heads, 2, rows)
-
-    gate_b = conv_proj[:, :channels].astype(jnp.float32)
-    gate_c = conv_proj[:, channels : 2 * channels].astype(jnp.float32)
-    conv_in = conv_proj[:, 2 * channels :].astype(jnp.float32)
-    u_vals = (gate_c * conv_in).astype(jnp.bfloat16)
-    edge = from_behind(u_vals[rows - (taps_count - 1) :], "sp", 1)
-    padded = jnp.concatenate([edge, u_vals], axis=0).astype(jnp.float32)
-    conv = conv_taps[0] * padded[0:rows]
-    for tap in range(1, taps_count):
-        conv = conv + conv_taps[tap] * padded[tap : tap + rows]
-    gated = gate_b * conv
-    grouped = rms_scale(gated.reshape(rows, channels // GROUP, GROUP)).reshape(rows, channels)
-    conv_out = (grouped * conv_gain).astype(jnp.bfloat16)
+    )(qn, kv, lambdas, sub_gain[:, None], conv_proj, conv_taps, conv_gain[None])
 
     piece = pltpu.VMEM((CHUNKS, own, width // CHUNKS), jnp.bfloat16)
     mixed = pl.pallas_call(

time: 111 us -> 101 us (0.910)
  other arithmetic: 5.11 us -> 0.59 us
  starting transfers between devices: 3.4 us -> 0 us
  local copies, waits for them, and re-layouts: 8.27 us -> 5.24 us
  Pallas kernels: 92.6 us -> 94.5 us
    ppermute x1 -> x0, starting transfers between devices: 3.4 us -> none  [from_behind(): return lax.ppermute(shard, axis, pairs)]
    convert_element_type x4 -> x0, other arithmetic: 2.85 us -> none  [the longest x1 1.17 us: on_device(): u_vals = (gate_c * conv_in).astype(jnp.bfloat16)]
    mul x13 -> x1, local copies, waits for them, and re-layouts: 1.5 us -> 0.08 us  [on_device(): query_gain.reshape(-1) * comp ** (-0.5)]
    reshape x1 -> x0, local copies, waits for them, and re-layouts: 1.31 us -> none  [on_device(): log_sums = logs.reshape(heads, 2, rows)]
    mul x2 -> x1, other arithmetic: 1.24 us -> 0.01 us  [on_device(): query_gain.reshape(-1) * comp ** (-0.5)]
    pallas_call x1, Pallas kernels: 18.8 us -> 19.9 us  [on_device(): pl.pallas_call(functools.partial(gather_project, comp), out_shape=(jax.Sh...]
    unnamed x13 -> x10, local copies, waits for them, and re-layouts: 4.7 us -> 4.33 us
  transfers between devices with their start and end apart: 1 -> 0, of which waited for: 0 -> 0; matrix products, arithmetic and copies ran while one was open for 5% -> 0% of each run, Pallas kernels for 50% -> 0%
where the time goes in v2:
time: 101 us
  Pallas kernels  94.5 us (94%)
  local copies, waits for them, and re-layouts  5.24 us (5%)
    pallas_call x1, Pallas kernels, on_device(): pl.pallas_call(functools.partial(attend, heads), out_shape=(jax.ShapeDtyp...  55.9 us
    pallas_call x1, Pallas kernels, on_device(): pl.pallas_call(functools.partial(gather_project, comp), out_shape=(jax.Sh...  19.9 us
    pallas_call x1, Pallas kernels, on_device(): pl.pallas_call(project_scatter, out_shape=jax.ShapeDtypeStruct((own, widt...  18.7 us
    unnamed x10, local copies, waits for them, and re-layouts  4.33 us

profile of v2, /device:TPU:24, one launch (start us, length us, event | category | flops | bytes accessed | tf_op | source)
XLA Modules:
  0.0 101.0 jit_solution(5281465469342993662)
XLA Ops:
  0.6 0.0 copy-start.3
  0.6 0.7 copy-done.3
  1.3 0.1 tile.14
  1.4 0.0 copy-start.1
  1.4 0.7 copy-done.1
  2.1 0.1 mul.15
  2.2 0.0 copy-start.2
  2.2 0.6 pad_maximum_fusion.qk_ref
  2.8 0.1 copy-done.2
  2.8 0.7 copy.18.sub_ref
  3.6 19.9 %gather_project.1 = (bf16[512,256]{1,0:T(8,128)(2,1)}, bf16[512,512]{1,0:T(8,128)(2,1)}, bf16[512,768]{1,0:T(8,128)(2,1)}) custom-call(bf16[128,2048]{1,0:T(8,128)(2,1)} %x_ref.1, f32[1,2048]{1,0:T(1,128)} %bitcast.5, f32[2,256]{1,0:T(2,128)} %pad_maximum_fusion.qk_ref, bf16[2048,256]{1,0:T(8,128)(2,1)} %rest_0_.1, bf16[2048,256]{1,0:T(8,128)(2,1)} %rest_1_.1, ...), custom_call_target="tpu_custom_call" | custom-call | tf_op jit(solution)/shard_map/gather_project/pallas_call | solution.py:397
  23.5 55.9 %attend.1 = (bf16[512,256]{1,0:T(8,128)(2,1)}, f32[2,2,512]{2,1,0:T(2,128)}, bf16[512,256]{1,0:T(8,128)(2,1)}) custom-call(bf16[512,256]{1,0:T(8,128)(2,1)} %get-tuple-element.8.q_ref, bf16[512,512]{1,0:T(8,128)(2,1)} %get-tuple-element.9.kv_ref, f32[2]{0:T(128)} %lam_ref.1, f32[128,1]{1,0:T(8,128)} %copy.18.sub_ref, ...), custom_call_target="tpu_custom_call" | custom-call | flops 20000000000 | tf_op jit(solution)/shard_map/attend/pallas_call | solution.py:415
  79.4 18.7 %project_scatter.1 = f32[128,2048]{1,0:T(8,128)} custom-call(bf16[512,256]{1,0:T(8,128)(2,1)} %get-tuple-element.11.heads_ref, bf16[512,256]{1,0:T(8,128)(2,1)} %get-tuple-element.12.conv_ref, bf16[256,2048]{1,0:T(8,128)(2,1)} %wa_ref.1, bf16[256,2048]{1,0:T(8,128)(2,1)} %wc_ref.1), custom_call_target="tpu_custom_call" | custom-call | tf_op jit(solution)/shard_map/project_scatter/pallas_call | solution.py:440
  98.1 0.0 copy-start
  98.1 2.3 %copy.21 = f32[128,2048]{1,0:T(8,128)} copy(f32[128,2048]{1,0:T(8,128)} %project_scatter.1) | data formatting | bytes 2097152
  100.4 0.0 copy-done
  100.4 0.6 copy.22
  (3 shorter events, 0.0 us)
Async XLA Ops:
  0.6 0.7 copy-start.3
  1.4 0.7 copy-start.1
  2.2 0.7 copy-start.2
  98.1 2.3 %copy-start = (f32[2,2,512]{2,1,0:T(2,128)S(1)}, f32[2,2,512]{2,1,0:T(2,128)}, u32[]{:S(2)}) copy-start(f32[2,2,512]{2,1,0:T(2,128)} %get-tuple-element.17) | copy-start | bytes 24580
